TPU v7x, 32 devices: a whole 2x2x4 slice. The times are simulated.
32 devices in a mesh: sp: 8 (over z, core), tp: 4 (over y, x).
Axes of the slice: x: 2, y: 2, z: 4, core: 2. Of those that a mesh axis runs over, the one named last changes fastest.
Arguments:
- prompt: bfloat16 [8, 2048, 2048], P('tp', 'sp'), may hold values from -6 to 6
- input_gain: float32 [2048], replicated, may hold values from 0.1 to 1.9
- key_weight: bfloat16 [1024, 2048], P('tp'), may hold values from -0.125 to 0.125
- value_weight: bfloat16 [1024, 2048], P('tp'), may hold values from -0.125 to 0.125
- key_gain: float32 [64], replicated, may hold values from 0.1 to 1.9
- queries: bfloat16 [8, 2, 1024], P('sp', None, 'tp'), may hold values from -6 to 6
- score_bias: float32 [2, 16], replicated, may hold values from -9 to -2
Outputs:
- keys: bfloat16 [8, 1024, 2048], P('sp', 'tp')
- values: bfloat16 [8, 1024, 2048], P('sp', 'tp')
- first_read: bfloat16 [8, 2, 1024], P('sp', None, 'tp')
All inputs are finite; a program needn't handle non-finite values.
Results may differ from a plain program's by a relative error of at most 0.01.
Values may be sent and summed in bfloat16 or wider, within the bound.
No kernel may reach another device: no remote copies, remote signals or barrier semaphores. Data moves between devices by JAX's collectives and lax.ppermute only.
A program may use at most 64 MiB of HBM per device.

v0:
```python
import math
import jax
import jax.numpy as jnp
from jax import lax
from jax.sharding import PartitionSpec as P

HEAD = 64
epsilon = 1e-06


def local(prompt, input_gain, key_weight, value_weight, key_gain, queries, score_bias):
    seq_here, pos_here, width = prompt.shape
    flat = prompt.astype(jnp.float32)
    normed = (
        flat * lax.rsqrt(jnp.mean(flat * flat, axis=-1, keepdims=True) + epsilon) * input_gain
    ).astype(jnp.bfloat16)
    stacked = jnp.stack([key_weight, value_weight])
    columns = key_weight.shape[0]
    kv_width = columns * lax.axis_size("tp")
    projected = jnp.einsum(
        "spd,knd->sknp",
        normed,
        lax.all_gather(stacked, "tp", axis=1, tiled=True),
        preferred_element_type=jnp.float32,
    )
    key_raw = projected[:, 0].reshape(seq_here, kv_width // HEAD, HEAD, pos_here)
    key_norm = (
        key_raw
        * lax.rsqrt(jnp.mean(key_raw * key_raw, axis=2, keepdims=True) + epsilon)
        * key_gain[:, None]
    )
    key_rows = key_norm.reshape(seq_here, kv_width, pos_here).astype(jnp.bfloat16)
    value_rows = projected[:, 1].astype(jnp.bfloat16)
    packed = jnp.stack([key_rows, value_rows], axis=1)
    by_sequence = lax.all_to_all(
        lax.all_to_all(packed, "tp", split_axis=2, concat_axis=0, tiled=True),
        "sp",
        split_axis=0,
        concat_axis=3,
        tiled=True,
    )
    keys = by_sequence[:, 0]
    values = by_sequence[:, 1]
    length = keys.shape[2]
    group = queries.shape[1]
    heads_here = columns // HEAD
    query_heads = queries[0].reshape(group, heads_here, HEAD)
    cache_keys = keys[0].reshape(heads_here, HEAD, length)
    scores = jnp.einsum("ghd,hds->ghs", query_heads, cache_keys, preferred_element_type=jnp.float32)
    first_head = lax.axis_index("tp") * heads_here
    offsets = lax.dynamic_slice_in_dim(score_bias, first_head, heads_here, 1)
    scores = scores / math.sqrt(HEAD) + offsets[:, :, None]
    log_break = jax.nn.log_sigmoid(scores)
    log_keep = jax.nn.log_sigmoid(-scores)
    later = lax.cumsum(log_keep, axis=2, reverse=True) - log_keep
    weights = jnp.exp(log_break + later).astype(jnp.bfloat16)
    cache_values = values[0].reshape(heads_here, HEAD, length)
    first_read = jnp.einsum(
        "ghs,hds->ghd", weights, cache_values, preferred_element_type=jnp.float32
    )
    first_read = first_read.astype(jnp.bfloat16).reshape(1, group, columns)
    return (keys, values, first_read)


def solution(mesh):
    placed = (P("tp", "sp", None), P(), P("tp", None), P("tp", None), P(), P("sp", None, "tp"), P())
    return jax.shard_map(
        local,
        mesh=mesh,
        in_specs=placed,
        out_specs=(P("sp", "tp", None), P("sp", "tp", None), P("sp", None, "tp")),
        check_vma=False,
    )
```

profile of v0, /device:TPU:0, one launch (start us, length us, event | category | flops | bytes accessed | tf_op | source)
XLA Modules:
  0.0 230.0 jit_solution(6662935200432588919)
XLA Ops:
  7.2 3.1 %pad_maximum_fusion = bf16[2,256,2048]{2,1,0:T(8,128)(2,1)} fusion(bf16[1,256,2048]{2,1,0:T(8,128)(2,1)} %bitcast.54, bf16[1,256,2048]{2,1,0:T(8,128)(2,1)} %bitcast.55), kind=kLoop, calls=%fused_computation.13 | loop fusion | flops 1048576 | bytes 4194304 | tf_op jit(solution)/shard_map/stack | solution.py:17
  10.4 0.6 copy-done.7
  11.1 0.9 copy-done.5
  11.9 0.5 fusion.2
  12.4 88.3 %all-gather.2.cloned.1.call-done = bf16[2,1024,2048]{2,1,0:T(8,128)(2,1)} async-done(((bf16[2,256,2048]{2,1,0:T(8,128)(2,1)}), bf16[2,1024,2048]{2,1,0:T(8,128)(2,1)}) %all-gather.2.cloned.1.call-update) | async-done | bytes 8388624 | tf_op jit(solution)/shard_map/all_gather | solution.py:23
  100.7 7.1 %fusion.7 = f32[2,2,1024,256]{3,2,0,1:T(8,128)S(1)} fusion(bf16[2,1024,2048]{2,1,0:T(8,128)(2,1)} %all-gather.2.cloned.1.call-done, bf16[2,256,2048]{2,1,0:T(8,128)(2,1)S(1)} %copy-done.5, f32[2048]{0:T(1024)S(1)} %copy-done.8, f32[2,256]{1,0:T(2,128)S(1)} %add_rsqrt_fusion.1), kind=kOutput, calls=%fused_computation.10 | convolution fusion | flops 4299161600 | bytes 14690304 | tf_op jit(solution)/shard_map/spd,knd->sknp/dot_general | solution.py:20
  108.0 1.8 copy-done.2
  110.2 1.9 fusion.13
  112.2 2.2 copy.42
  114.4 28.0 %all_to_all.36 = bf16[2,2,1024,256]{3,0,1,2:T(2,128)(2,1)S(1)} all-to-all(bf16[2,2,1024,256]{3,0,1,2:T(2,128)(2,1)S(1)} %copy.42), channel_id=1, replica_groups=mesh['sp'=8,'tp'=4] {'tp'}, dimensions={2} | all-to-all | bytes 4194304 | tf_op jit(solution)/shard_map/all_to_all | solution.py:36
  142.6 1.5 copy.44
  144.1 4.7 %all-to-all-start.1 = ((bf16[8,2,256,256]{3,2,1,0:T(8,128)(2,1)}), bf16[8,2,256,256]{3,2,1,0:T(8,128)(2,1)S(1)}, u32[]{:S(2)}, u32[]{:S(2)}) async-start(bf16[8,2,256,256]{3,2,1,0:T(8,128)(2,1)} %bitcast.49), calls=%async_computation.1 | async-start | bytes 4194304 | tf_op jit(solution)/shard_map/all_to_all | solution.py:35
  149.1 48.8 %all-to-all-done.1 = bf16[8,2,256,256]{3,2,1,0:T(8,128)(2,1)S(1)} async-done(((bf16[8,2,256,256]{3,2,1,0:T(8,128)(2,1)}), bf16[8,2,256,256]{3,2,1,0:T(8,128)(2,1)S(1)}, u32[]{:S(2)}, u32[]{:S(2)}) %all-to-all-start.1) | async-done | bytes 2097184 | tf_op jit(solution)/shard_map/all_to_all | solution.py:35
  197.9 1.3 copy-done.1
  199.2 2.8 %copy.45 = bf16[1,2,256,8,256]{2,4,3,1,0:T(8,128)(2,1)S(1)} copy(bf16[1,2,256,8,256]{4,2,1,3,0:T(8,128)(2,1)} %bitcast.48) | data formatting | bytes 4194304 | tf_op jit(solution)/shard_map/all_to_all | solution.py:35
  202.1 1.8 fusion.27
  203.9 1.6 copy.47
  205.8 9.9 %reduce-window.6 = f32[2,4,16,128]{3,2,1,0:T(8,128)S(1)} reduce-window(f32[2,4,16,128]{3,2,1,0:T(8,128)S(1)} %copy.50, f32[]{:T(128)} %constant.9.clone.1), window={size=1x1x1x128 pad=0_0x0_0x0_0x0_127}, to_apply=%region_2.3 | reduce-window | flops 2080768 | bytes 131076 | tf_op jit(solution)/shard_map/reduce-window
  215.9 0.4 reduce-window.9
  216.5 1.4 copy.46
  217.9 1.7 fusion.16
  219.7 0.6 reshape.46
  220.3 1.4 copy.53
  221.7 1.4 copy.54
  (36 shorter events, 2.0 us)
Async XLA Ops:
  7.2 141.7 %copy-start = (f32[2,16]{1,0:T(2,128)S(1)}, f32[2,16]{1,0:T(2,128)}, u32[]{:S(2)}) copy-start(f32[2,16]{1,0:T(2,128)} %param.13) | copy-start | bytes 388
  7.2 93.5 %all-gather.2.cloned.1.call-start = ((), (), s32[]{:S(2)}) async-start(), calls=%async_computation.2 | async-start | bytes 10485760 | tf_op jit(solution)/shard_map/all_gather | solution.py:23
  10.3 0.7 copy-start.7
  10.3 1.6 copy-start.5
  10.3 90.4 %copy-start.8 = (f32[2048]{0:T(1024)S(1)}, f32[2048]{0:T(1024)}, u32[]{:S(2)}) copy-start(f32[2048]{0:T(1024)} %param.8) | copy-start | bytes 24580
  107.9 1.9 copy-start.2
  144.1 4.9 %copy-start.6 = (bf16[1,2,256]{2,1,0:T(2,128)(2,1)S(1)}, bf16[1,2,256]{2,1,0:T(2,128)(2,1)}, u32[]{:S(2)}) copy-start(bf16[1,2,256]{2,1,0:T(2,128)(2,1)} %param.12) | copy-start | bytes 3076
  144.1 53.8 %all-to-all-start.1 = ((bf16[8,2,256,256]{3,2,1,0:T(8,128)(2,1)}), bf16[8,2,256,256]{3,2,1,0:T(8,128)(2,1)S(1)}, u32[]{:S(2)}, u32[]{:S(2)}) async-start(bf16[8,2,256,256]{3,2,1,0:T(8,128)(2,1)} %bitcast.49), calls=%async_computation.1 | async-start | bytes 4194304 | tf_op jit(solution)/shard_map/all_to_all | solution.py:35
  197.9 1.3 copy-start.1
  203.9 12.6 %copy-start.4 = (bf16[1,1,256,2048]{2,3,1,0:T(8,128)(2,1)S(1)}, bf16[1,1,256,2048]{2,3,1,0:T(8,128)(2,1)}, u32[]{:S(2)}) copy-start(bf16[1,1,256,2048]{2,3,1,0:T(8,128)(2,1)} %get-tuple-element.15) | copy-start | bytes 3145732
  216.5 3.8 %copy-start.3 = (bf16[1,256,2048]{1,2,0:T(8,128)(2,1)S(1)}, bf16[1,256,2048]{1,2,0:T(8,128)(2,1)}, u32[]{:S(2)}) copy-start(bf16[1,256,2048]{1,2,0:T(8,128)(2,1)} %get-tuple-element.13) | copy-start | bytes 3145732
Sparse Core Ops, SparseCore 0:
  10.5 90.1 all-gather.1
where the time goes:
time: 230 us
  waiting for transfers between devices  137 us (60%)
  blocking collectives  28 us (12%)
  local copies, waits for them, and re-layouts  20.4 us (9%)
  other arithmetic  16.4 us (7%)
  between operations  14.2 us (6%)
  matrix products  9.17 us (4%)
  starting transfers between devices  4.77 us (2%)
    all_gather x1, waiting for transfers between devices, local(): lax.all_gather(stacked, 'tp', axis=1, tiled=True)  88.3 us
    all_to_all x1, waiting for transfers between devices, local(): lax.all_to_all(lax.all_to_all(packed, 'tp', split_axis=2, concat_axis=0,...  48.8 us
    all_to_all x1, blocking collectives, local(): lax.all_to_all(packed, 'tp', split_axis=2, concat_axis=0, tiled=True)  28 us
    another operation x2, other arithmetic  10.3 us
    unnamed x20, local copies, waits for them, and re-layouts  7.48 us
    dot_general x1, matrix products, local(): jnp.einsum('spd,knd->sknp', normed, lax.all_gather(stacked, 'tp', axis=1,...  7.13 us
    all_to_all x1, starting transfers between devices, local(): lax.all_to_all(lax.all_to_all(packed, 'tp', split_axis=2, concat_axis=0,...  4.73 us
  transfers between devices with their start and end apart: 2, of which 2 were waited for; matrix products, arithmetic and copies ran while one was open for 0% of the time, Pallas kernels for 0%

commit v1 on v0

--- a/solution.py
+++ b/solution.py
@@ -33,7 +33,10 @@
     value_rows = projected[:, 1].astype(jnp.bfloat16)
     packed = jnp.stack([key_rows, value_rows], axis=1)
     by_sequence = lax.all_to_all(
-        lax.all_to_all(packed, "tp", split_axis=2, concat_axis=0, tiled=True),
+        jnp.concatenate(
+            lax.all_to_all(jnp.stack(jnp.split(packed, lax.axis_size("tp"), axis=2)), "tp", 0, 0),
+            axis=0,
+        ),
         "sp",
         split_axis=0,
         concat_axis=3,

time: 230 us -> 228 us (level)
  local copies, waits for them, and re-layouts: 20.4 us -> 17.9 us
    all_to_all x3 -> x2, local copies, waits for them, and re-layouts: 4.61 us -> 4.33 us  [the longest x1 2.85 us: local(): lax.all_to_all(jnp.concatenate(lax.all_to_all(jnp.stack(jnp.split(packed,...]
    another operation x3 -> x4, other arithmetic: 10.5 us -> 10.8 us
where the time goes in v1:
time: 228 us
  waiting for transfers between devices  137 us (60%)
  blocking collectives  28 us (12%)
  local copies, waits for them, and re-layouts  17.9 us (8%)
  other arithmetic  16.7 us (7%)
  between operations  14.2 us (6%)
  matrix products  9.17 us (4%)
  starting transfers between devices  4.77 us (2%)
    all_gather x1, waiting for transfers between devices, local(): lax.all_gather(stacked, 'tp', axis=1, tiled=True)  88.3 us
    all_to_all x1, waiting for transfers between devices, local(): lax.all_to_all(jnp.concatenate(lax.all_to_all(jnp.stack(jnp.split(packed,...  48.8 us
    all_to_all x1, blocking collectives, local(): lax.all_to_all(jnp.stack(jnp.split(packed, lax.axis_size('tp'), axis=2)),...  28 us
    another operation x2, other arithmetic  10.3 us
    unnamed x20, local copies, waits for them, and re-layouts  7.48 us
    dot_general x1, matrix products, local(): jnp.einsum('spd,knd->sknp', normed, lax.all_gather(stacked, 'tp', axis=1,...  7.12 us
    all_to_all x1, starting transfers between devices, local(): lax.all_to_all(jnp.concatenate(lax.all_to_all(jnp.stack(jnp.split(packed,...  4.74 us
  transfers between devices with their start and end apart: 2, of which 2 were waited for; matrix products, arithmetic and copies ran while one was open for 0% of the time, Pallas kernels for 0%

profile of v1, /device:TPU:0, one launch (start us, length us, event | category | flops | bytes accessed | tf_op | source)
XLA Modules:
  0.0 227.8 jit_solution(5218365780117662683)
XLA Ops:
  7.2 3.1 %pad_maximum_fusion = bf16[2,256,2048]{2,1,0:T(8,128)(2,1)} fusion(bf16[1,256,2048]{2,1,0:T(8,128)(2,1)} %bitcast.58, bf16[1,256,2048]{2,1,0:T(8,128)(2,1)} %bitcast.59), kind=kLoop, calls=%fused_computation.19 | loop fusion | flops 1048576 | bytes 4194304 | tf_op jit(solution)/shard_map/stack | solution.py:17
  10.4 0.6 copy-done.7
  11.1 0.9 copy-done.5
  11.9 0.5 fusion.2
  12.4 88.3 %all-gather.2.cloned.1.call-done = bf16[2,1024,2048]{2,1,0:T(8,128)(2,1)} async-done(((bf16[2,256,2048]{2,1,0:T(8,128)(2,1)}), bf16[2,1024,2048]{2,1,0:T(8,128)(2,1)}) %all-gather.2.cloned.1.call-update) | async-done | bytes 8388624 | tf_op jit(solution)/shard_map/all_gather | solution.py:23
  100.7 7.1 %fusion.7 = f32[2,2,1024,256]{3,2,0,1:T(8,128)S(1)} fusion(bf16[2,1024,2048]{2,1,0:T(8,128)(2,1)} %all-gather.2.cloned.1.call-done, bf16[2,256,2048]{2,1,0:T(8,128)(2,1)S(1)} %copy-done.5, f32[2048]{0:T(1024)S(1)} %copy-done.8, f32[2,256]{1,0:T(2,128)S(1)} %add_rsqrt_fusion.1), kind=kOutput, calls=%fused_computation.16 | convolution fusion | flops 4299161600 | bytes 14690304 | tf_op jit(solution)/shard_map/spd,knd->sknp/dot_general | solution.py:20
  108.0 1.8 copy-done.2
  110.1 1.9 fusion.13
  112.4 28.0 %all_to_all.23 = bf16[4,2,2,256,256]{4,3,1,2,0:T(8,128)(2,1)S(1)} all-to-all(bf16[4,2,2,256,256]{4,3,1,2,0:T(8,128)(2,1)S(1)} %pad_maximum_fusion.1), channel_id=1, replica_groups=mesh['sp'=8,'tp'=4] {'tp'}, dimensions={0} | all-to-all | bytes 4194304 | tf_op jit(solution)/shard_map/all_to_all | solution.py:37
  140.4 1.5 copy.20
  141.9 4.7 %all-to-all-start.1 = ((bf16[8,2,256,256]{3,2,1,0:T(8,128)(2,1)}), bf16[8,2,256,256]{3,2,1,0:T(8,128)(2,1)S(1)}, u32[]{:S(2)}, u32[]{:S(2)}) async-start(bf16[8,2,256,256]{3,2,1,0:T(8,128)(2,1)} %bitcast.54), calls=%async_computation.1 | async-start | bytes 4194304 | tf_op jit(solution)/shard_map/all_to_all | solution.py:35
  146.9 48.8 %all-to-all-done.1 = bf16[8,2,256,256]{3,2,1,0:T(8,128)(2,1)S(1)} async-done(((bf16[8,2,256,256]{3,2,1,0:T(8,128)(2,1)}), bf16[8,2,256,256]{3,2,1,0:T(8,128)(2,1)S(1)}, u32[]{:S(2)}, u32[]{:S(2)}) %all-to-all-start.1) | async-done | bytes 2097184 | tf_op jit(solution)/shard_map/all_to_all | solution.py:35
  195.7 1.3 copy-done.1
  197.0 2.8 %copy.21 = bf16[1,2,256,8,256]{2,4,3,1,0:T(8,128)(2,1)S(1)} copy(bf16[1,2,256,8,256]{4,2,1,3,0:T(8,128)(2,1)} %bitcast.53) | data formatting | bytes 4194304 | tf_op jit(solution)/shard_map/all_to_all | solution.py:35
  199.9 1.8 fusion.34
  201.7 1.6 copy.23
  203.2 0.3 fusion.27
  203.6 9.9 %reduce-window.6 = f32[2,4,16,128]{3,2,1,0:T(8,128)S(1)} reduce-window(f32[2,4,16,128]{3,2,1,0:T(8,128)S(1)} %copy.26, f32[]{:T(128)} %constant.9.clone.1), window={size=1x1x1x128 pad=0_0x0_0x0_0x0_127}, to_apply=%region_2.3 | reduce-window | flops 2080768 | bytes 131076 | tf_op jit(solution)/shard_map/reduce-window
  213.7 0.4 reduce-window.9
  214.3 1.4 copy.22
  215.7 1.7 fusion.16
  217.5 0.6 reshape.50
  218.1 1.4 copy.29
  219.5 1.4 copy.30
  (35 shorter events, 1.7 us)
Async XLA Ops:
  7.2 139.5 %copy-start = (f32[2,16]{1,0:T(2,128)S(1)}, f32[2,16]{1,0:T(2,128)}, u32[]{:S(2)}) copy-start(f32[2,16]{1,0:T(2,128)} %param.13) | copy-start | bytes 388
  7.2 93.5 %all-gather.2.cloned.1.call-start = ((), (), s32[]{:S(2)}) async-start(), calls=%async_computation.2 | async-start | bytes 10485760 | tf_op jit(solution)/shard_map/all_gather | solution.py:23
  10.3 0.7 copy-start.7
  10.3 1.6 copy-start.5
  10.3 90.4 %copy-start.8 = (f32[2048]{0:T(1024)S(1)}, f32[2048]{0:T(1024)}, u32[]{:S(2)}) copy-start(f32[2048]{0:T(1024)} %param.8) | copy-start | bytes 24580
  107.9 1.9 copy-start.2
  141.9 4.9 %copy-start.6 = (bf16[1,2,256]{2,1,0:T(2,128)(2,1)S(1)}, bf16[1,2,256]{2,1,0:T(2,128)(2,1)}, u32[]{:S(2)}) copy-start(bf16[1,2,256]{2,1,0:T(2,128)(2,1)} %param.12) | copy-start | bytes 3076
  141.9 53.8 %all-to-all-start.1 = ((bf16[8,2,256,256]{3,2,1,0:T(8,128)(2,1)}), bf16[8,2,256,256]{3,2,1,0:T(8,128)(2,1)S(1)}, u32[]{:S(2)}, u32[]{:S(2)}) async-start(bf16[8,2,256,256]{3,2,1,0:T(8,128)(2,1)} %bitcast.54), calls=%async_computation.1 | async-start | bytes 4194304 | tf_op jit(solution)/shard_map/all_to_all | solution.py:35
  195.7 1.3 copy-start.1
  201.7 12.6 %copy-start.4 = (bf16[1,1,256,2048]{2,3,1,0:T(8,128)(2,1)S(1)}, bf16[1,1,256,2048]{2,3,1,0:T(8,128)(2,1)}, u32[]{:S(2)}) copy-start(bf16[1,1,256,2048]{2,3,1,0:T(8,128)(2,1)} %get-tuple-element.9) | copy-start | bytes 3145732
  214.3 3.8 %copy-start.3 = (bf16[1,256,2048]{1,2,0:T(8,128)(2,1)S(1)}, bf16[1,256,2048]{1,2,0:T(8,128)(2,1)}, u32[]{:S(2)}) copy-start(bf16[1,256,2048]{1,2,0:T(8,128)(2,1)} %get-tuple-element.7) | copy-start | bytes 3145732
Sparse Core Ops, SparseCore 0:
  10.5 90.1 all-gather.1
